TPU v7x, 32 devices: a whole 2x2x4 slice. The times are simulated.
32 devices in a mesh: fs: 4 (over z), rep: 4 (over y, x), tp: 2 (over core).
Axes of the slice: x: 2, y: 2, z: 4, core: 2. Of those that a mesh axis runs over, the one named last changes fastest.
Arguments:
- saved_input: bfloat16 [16384, 2048], P(('fs', 'rep')), may hold values from -6 to 6
- value_cotangent: bfloat16 [16384, 4096], P(('fs', 'rep'), 'tp'), may hold values from -0.0061950684 to 0.0061950684
- factor: bfloat16 [2048, 128], P('fs'), may hold values from -1.5 to 1.5
- weight: float32 [2048, 4096], P('fs', 'tp'), may hold values from -1.2 to 1.2
- first_moment: float32 [128, 4096], P('fs', 'tp'), may hold values from -1.8 to 1.8
- second_moment: float32 [128, 4096], P('fs', 'tp'), may hold values from 0.1 to 1
Outputs:
- low_grad: float32 [128, 4096], P('fs', 'tp')
- new_first: float32 [128, 4096], P('fs', 'tp')
- new_second: float32 [128, 4096], P('fs', 'tp')
- direction: float32 [2048, 4096], P('fs', 'tp')
- new_weight: float32 [2048, 4096], P('fs', 'tp')
- new_copy: bfloat16 [2048, 4096], P('fs', 'tp')
All inputs are finite; a program needn't handle non-finite values.
Results may differ from a plain program's by a relative error of at most 0.006.
Values may be sent and summed in bfloat16 or wider, within the bound.
A program may use at most 64 MiB of HBM per device.

v0:
```python
import jax
import jax.numpy as jnp
from jax import lax
from jax.sharding import PartitionSpec as P

D = 2048
E = 4096
first_decay = 0.9
second_decay = 0.9
learn_rate = 0.05
epsilon = 1e-08


def on_device(saved_input, value_cotangent, factor, weight, first_moment, second_moment):
    factor_wide = factor.astype(jnp.float32)
    factor_whole = lax.all_gather(factor, "fs", axis=0, tiled=True)
    projected = jnp.dot(saved_input, factor_whole, preferred_element_type=jnp.float32)
    upper = projected.astype(jnp.bfloat16)
    lower = (projected - upper.astype(jnp.float32)).astype(jnp.bfloat16)
    dims = (((0,), (0,)), ((), ()))
    high_part = lax.dot_general(upper, value_cotangent, dims, preferred_element_type=jnp.float32)
    low_part = lax.dot_general(lower, value_cotangent, dims, preferred_element_type=jnp.float32)
    low_grad = lax.psum_scatter(high_part + low_part, "fs", scatter_dimension=0, tiled=True)
    low_grad = lax.psum(low_grad, "rep")
    new_first = first_decay * first_moment + (1.0 - first_decay) * low_grad
    new_second = second_decay * second_moment + (1.0 - second_decay) * low_grad * low_grad
    ratio = new_first / (jnp.sqrt(new_second) + epsilon)
    ratio_whole = lax.all_gather(ratio, "fs", axis=0, tiled=True)
    raw = jnp.dot(factor_wide, ratio_whole, precision=lax.Precision.HIGHEST)
    total = lax.psum(jnp.sum(raw * raw), ("fs", "tp"))
    spread = jnp.sqrt(total / (D * E))
    direction = raw / (spread + 1.0)
    new_weight = weight - learn_rate * direction
    return (low_grad, new_first, new_second, direction, new_weight, new_weight.astype(jnp.bfloat16))


def solution(mesh):
    placed = (
        P(("fs", "rep"), None),
        P(("fs", "rep"), "tp"),
        P("fs", None),
        P("fs", "tp"),
        P("fs", "tp"),
        P("fs", "tp"),
    )
    return jax.shard_map(
        on_device,
        mesh=mesh,
        in_specs=placed,
        out_specs=(
            P("fs", "tp"),
            P("fs", "tp"),
            P("fs", "tp"),
            P("fs", "tp"),
            P("fs", "tp"),
            P("fs", "tp"),
        ),
        check_vma=False,
    )
```

profile of v0, /device:TPU:0, one launch (start us, length us, event | category | flops | bytes accessed | tf_op | source)
XLA Modules:
  0.0 185.3 jit_solution(11213346444921834174)
XLA Ops:
  7.2 0.0 reduce-scatter.2.cloned.1.call-start
  7.2 0.0 copy-start
  7.2 17.7 %all_gather.6 = bf16[2048,128]{1,0:T(8,128)(2,1)S(1)} all-gather(bf16[512,128]{1,0:T(8,128)(2,1)} %param.8), channel_id=1, replica_groups=mesh['fs'=4,'rep'=4,'tp'=2] {'fs'}, dimensions={0}, use_global_device_ids=true | all-gather | bytes 655360 | tf_op jit(solution)/shard_map/all_gather | solution.py:16
  24.9 3.4 %fusion.6 = f32[1024,128]{1,0:T(8,128)S(1)} fusion(bf16[1024,2048]{1,0:T(8,128)(2,1)} %param.6, bf16[2048,128]{1,0:T(8,128)(2,1)S(1)} %all_gather.6), kind=kOutput, calls=%fused_computation.13 | convolution fusion | flops 536870912 | bytes 5242880 | tf_op jit(solution)/shard_map/dot_general | solution.py:17
  28.4 0.0 copy-done
  28.4 0.7 fusion.2
  29.1 0.0 copy-start.3
  29.1 0.0 copy-start.4
  29.2 1.7 convolution_add_fusion
  30.9 0.0 reduce-scatter.2.cloned.1.call-update
  30.9 0.0 all-reduce.2.cloned.1.call-start
  31.0 29.2 %reduce-scatter.2.cloned.1.call-done = f32[32,2048]{1,0:T(8,128)} async-done(((f32[128,2048]{1,0:T(8,128)}), f32[32,2048]{1,0:T(8,128)}) %reduce-scatter.2.cloned.1.call-update) | async-done | bytes 262160 | tf_op jit(solution)/shard_map/reduce_scatter | solution.py:23
  60.1 0.0 all-reduce.2.cloned.1.call-update
  60.1 0.0 all-gather.2.cloned.1.call-start
  60.2 44.5 %all-reduce.2.cloned.1.call-done = f32[32,2048]{1,0:T(8,128)} async-done(((f32[32,2048]{1,0:T(8,128)}), f32[32,2048]{1,0:T(8,128)}) %all-reduce.2.cloned.1.call-update) | async-done | bytes 262160 | tf_op jit(solution)/shard_map/psum | solution.py:24
  104.6 0.0 copy-done.3
  104.6 0.0 copy-done.4
  104.6 1.9 %add_divide_fusion = (f32[32,2048]{1,0:T(8,128)}, f32[32,2048]{1,0:T(8,128)}, f32[32,2048]{1,0:T(8,128)}) fusion(f32[32,2048]{1,0:T(8,128)} %all-reduce.2.cloned.1.call-done, f32[32,2048]{1,0:T(8,128)S(1)} %copy-done.3, f32[32,2048]{1,0:T(8,128)S(1)} %copy-done.4), kind=kLoop, calls=%fused_computation.8 | loop fusion | flops 524288 | bytes 1572864 | tf_op jit(solution)/shard_map/div | solution.py:27
  106.5 0.0 all-gather.2.cloned.1.call-update
  106.6 0.0 copy-start.2
  106.6 5.4 %copy.12 = f32[512,2048]{0,1:T(8,128)} copy(f32[512,2048]{1,0:T(8,128)} %param.9) | data formatting | bytes 8388608 | tf_op args[3]
  112.0 22.8 %all-gather.2.cloned.1.call-done = f32[128,2048]{1,0:T(8,128)} async-done(((f32[32,2048]{1,0:T(8,128)}), f32[128,2048]{1,0:T(8,128)}) %all-gather.2.cloned.1.call-update) | async-done | bytes 1048592 | tf_op jit(solution)/shard_map/all_gather | solution.py:28
  134.8 0.0 copy-done.2
  134.8 6.0 %multiply_reduce_fusion = (f32[]{:T(128)}, f32[2048,512]{1,0:T(8,128)}) fusion(f32[128,2048]{1,0:T(8,128)} %all-gather.2.cloned.1.call-done, bf16[512,128]{1,0:T(8,128)(2,1)S(1)} %copy-done.2), kind=kOutput, calls=%fused_computation.2 | convolution fusion | flops 1612709888 | bytes 5373956 | tf_op jit(solution)/shard_map/dot_general | solution.py:29
  140.8 15.3 %psum.15 = f32[]{:T(128)} all-reduce(f32[]{:T(128)} %get-tuple-element.18), channel_id=1, replica_groups=mesh['fs'=4,'rep'=4,'tp'=2] {'fs','tp'}, use_global_device_ids=true, to_apply=%region_3.0 | all-reduce | flops 1 | bytes 8 | tf_op jit(solution)/shard_map/psum | solution.py:30
  156.7 8.3 %fusion.4 = (bf16[512,2048]{0,1:T(8,128)(2,1)S(1)}, f32[512,2048]{0,1:T(8,128)}, f32[512,2048]{0,1:T(8,128)}) fusion(f32[512,2048]{0,1:T(8,128)} %copy.12, f32[2048,512]{1,0:T(8,128)} %get-tuple-element.19, f32[]{:T(128)S(6)} %add.29), kind=kLoop, calls=%fused_computation.12 | loop fusion | flops 4194304 | bytes 18874372 | tf_op jit(solution)/shard_map/convert_element_type | solution.py:34
  165.0 2.4 %copy.15 = bf16[512,2048]{1,0:T(8,128)(2,1)} copy(bf16[512,2048]{0,1:T(8,128)(2,1)S(1)} %get-tuple-element.12) | data formatting | bytes 4194304
  167.4 5.3 %copy.14 = f32[512,2048]{1,0:T(8,128)} copy(f32[512,2048]{0,1:T(8,128)} %get-tuple-element.13) | data formatting | bytes 8388608
  172.7 0.0 copy-start.1
  172.7 5.4 %copy.13 = f32[512,2048]{1,0:T(8,128)} copy(f32[512,2048]{0,1:T(8,128)} %get-tuple-element.14) | data formatting | bytes 8388608
  178.1 0.0 copy-done.1
  178.1 0.7 copy.17
Async XLA Ops:
  7.2 52.9 %reduce-scatter.2.cloned.1.call-start = ((), (), s32[]{:S(2)}) async-start(), calls=%async_computation.1 | async-start | bytes 1310720 | tf_op jit(solution)/shard_map/reduce_scatter | solution.py:23
  7.2 21.2 %copy-start = (bf16[1024,2048]{1,0:T(8,128)(2,1)S(1)}, bf16[1024,2048]{1,0:T(8,128)(2,1)}, u32[]{:S(2)}) copy-start(bf16[1024,2048]{1,0:T(8,128)(2,1)} %param.7) | copy-start | bytes 12582916
  29.1 75.5 %copy-start.3 = (f32[32,2048]{1,0:T(8,128)S(1)}, f32[32,2048]{1,0:T(8,128)}, u32[]{:S(2)}) copy-start(f32[32,2048]{1,0:T(8,128)} %param.11) | copy-start | bytes 786436
  29.1 75.5 %copy-start.4 = (f32[32,2048]{1,0:T(8,128)S(1)}, f32[32,2048]{1,0:T(8,128)}, u32[]{:S(2)}) copy-start(f32[32,2048]{1,0:T(8,128)} %param.10) | copy-start | bytes 786436
  30.9 73.7 %all-reduce.2.cloned.1.call-start = ((), (), s32[]{:S(2)}) async-start(), calls=%async_computation.2 | async-start | bytes 524288 | tf_op jit(solution)/shard_map/psum | solution.py:24
  60.1 74.7 %all-gather.2.cloned.1.call-start = ((), (), s32[]{:S(2)}) async-start(), calls=%async_computation.3 | async-start | bytes 1310720 | tf_op jit(solution)/shard_map/all_gather | solution.py:28
  106.6 28.2 %copy-start.2 = (bf16[512,128]{1,0:T(8,128)(2,1)S(1)}, bf16[512,128]{1,0:T(8,128)(2,1)}, u32[]{:S(2)}) copy-start(bf16[512,128]{1,0:T(8,128)(2,1)} %param.8) | copy-start | bytes 393220
  172.7 5.4 %copy-start.1 = (f32[32,2048]{1,0:T(8,128)S(1)}, f32[32,2048]{1,0:T(8,128)}, u32[]{:S(2)}) copy-start(f32[32,2048]{1,0:T(8,128)} %all-reduce.2.cloned.1.call-done) | copy-start | bytes 786436
Sparse Core Ops, SparseCore 0:
  31.0 29.0 reduce-scatter.1
  63.0 41.5 all-reduce.1
  106.8 27.9 all-gather.1
where the time goes:
time: 186 us; the launch traced here: 185 us
  waiting for transfers between devices  96.5 us (52%)
  blocking collectives  33 us (18%)
  local copies, waits for them, and re-layouts  19.2 us (10%)
  between operations  14.5 us (8%)
  matrix products  11.9 us (6%)
  other arithmetic  10.2 us (5%)
    psum x1, waiting for transfers between devices, on_device(): low_grad = lax.psum(low_grad, 'rep')  44.5 us
    reduce_scatter x1, waiting for transfers between devices, on_device(): lax.psum_scatter(high_part + low_part, 'fs', scatter_dimension=0, tiled=T...  29.2 us
    all_gather x1, waiting for transfers between devices, on_device(): ratio_whole = lax.all_gather(ratio, 'fs', axis=0, tiled=True)  22.8 us
    unnamed x15, local copies, waits for them, and re-layouts  19.2 us
    all_gather x1, blocking collectives, on_device(): factor_whole = lax.all_gather(factor, 'fs', axis=0, tiled=True)  17.7 us
    psum x1, blocking collectives, on_device(): total = lax.psum(jnp.sum(raw * raw), ('fs', 'tp'))  15.3 us
    convert_element_type x1, other arithmetic, on_device(): new_weight.astype(jnp.bfloat16)  8.28 us
    dot_general x1, matrix products, on_device(): raw = jnp.dot(factor_wide, ratio_whole, precision=lax.Precision.HIGHEST)  5.95 us
  transfers between devices with their start and end apart: 3, of which 3 were waited for; matrix products, arithmetic and copies ran while one was open for 3% of the time, Pallas kernels for 0%

commit v1 on v0

--- a/solution.py
+++ b/solution.py
@@ -21,7 +21,7 @@
     high_part = lax.dot_general(upper, value_cotangent, dims, preferred_element_type=jnp.float32)
     low_part = lax.dot_general(lower, value_cotangent, dims, preferred_element_type=jnp.float32)
     low_grad = lax.psum_scatter(high_part + low_part, "fs", scatter_dimension=0, tiled=True)
-    low_grad = lax.psum(low_grad, "rep")
+    low_grad = jnp.sum(lax.all_gather(low_grad, "rep"), axis=0)
     new_first = first_decay * first_moment + (1.0 - first_decay) * low_grad
     new_second = second_decay * second_moment + (1.0 - second_decay) * low_grad * low_grad
     ratio = new_first / (jnp.sqrt(new_second) + epsilon)

time: 186 us -> 168 us (0.903)
  waiting for transfers between devices: 96.5 us -> 78.7 us
    psum x1 -> x0, waiting for transfers between devices: 44.5 us -> none  [on_device(): low_grad = lax.psum(low_grad, 'rep')]
    all_gather x0 -> x1, waiting for transfers between devices: none -> 26.8 us  [on_device(): low_grad = jnp.sum(lax.all_gather(low_grad, 'rep'), axis=0)]
    unnamed x15 -> x14, local copies, waits for them, and re-layouts: 19.2 us -> 18.5 us
where the time goes in v1:
time: 168 us; the launch traced here: 167 us
  waiting for transfers between devices  78.7 us (47%)
  blocking collectives  33 us (20%)
  local copies, waits for them, and re-layouts  18.5 us (11%)
  between operations  14.5 us (9%)
  matrix products  11.8 us (7%)
  other arithmetic  10.6 us (6%)
    reduce_scatter x1, waiting for transfers between devices, on_device(): lax.psum_scatter(high_part + low_part, 'fs', scatter_dimension=0, tiled=T...  29.2 us
    all_gather x1, waiting for transfers between devices, on_device(): low_grad = jnp.sum(lax.all_gather(low_grad, 'rep'), axis=0)  26.8 us
    all_gather x1, waiting for transfers between devices, on_device(): ratio_whole = lax.all_gather(ratio, 'fs', axis=0, tiled=True)  22.7 us
    unnamed x14, local copies, waits for them, and re-layouts  18.5 us
    all_gather x1, blocking collectives, on_device(): factor_whole = lax.all_gather(factor, 'fs', axis=0, tiled=True)  17.7 us
    psum x1, blocking collectives, on_device(): total = lax.psum(jnp.sum(raw * raw), ('fs', 'tp'))  15.3 us
    convert_element_type x1, other arithmetic, on_device(): new_weight.astype(jnp.bfloat16)  8.28 us
    dot_general x1, matrix products, on_device(): raw = jnp.dot(factor_wide, ratio_whole, precision=lax.Precision.HIGHEST)  5.95 us
  transfers between devices with their start and end apart: 3, of which 3 were waited for; matrix products, arithmetic and copies ran while one was open for 3% of the time, Pallas kernels for 0%

profile of v1, /device:TPU:0, one launch (start us, length us, event | category | flops | bytes accessed | tf_op | source)
XLA Modules:
  0.0 167.3 jit_solution(8018532814044504057)
XLA Ops:
  7.2 0.0 reduce-scatter.2.cloned.1.call-start
  7.2 0.0 copy-start
  7.2 17.7 %all_gather.12 = bf16[2048,128]{1,0:T(8,128)(2,1)S(1)} all-gather(bf16[512,128]{1,0:T(8,128)(2,1)} %param.8), channel_id=1, replica_groups=mesh['fs'=4,'rep'=4,'tp'=2] {'fs'}, dimensions={0}, use_global_device_ids=true | all-gather | bytes 655360 | tf_op jit(solution)/shard_map/all_gather | solution.py:16
  24.9 3.4 %fusion.6 = f32[1024,128]{1,0:T(8,128)S(1)} fusion(bf16[1024,2048]{1,0:T(8,128)(2,1)} %param.6, bf16[2048,128]{1,0:T(8,128)(2,1)S(1)} %all_gather.12), kind=kOutput, calls=%fused_computation.13 | convolution fusion | flops 536870912 | bytes 5242880 | tf_op jit(solution)/shard_map/dot_general | solution.py:17
  28.4 0.0 copy-done
  28.4 0.7 fusion.2
  29.1 0.0 copy-start.3
  29.1 0.0 copy-start.4
  29.2 1.7 %convolution_add_fusion = f32[128,2048]{1,0:T(8,128)} fusion(f32[128,2048]{1,0:T(8,128)S(1)} %fusion.2, bf16[1024,2048]{1,0:T(8,128)(2,1)S(1)} %copy-done, f32[1024,128]{1,0:T(8,128)S(1)} %fusion.6), kind=kOutput, calls=%fused_computation.3 | convolution fusion | flops 537657344 | bytes 6815744 | tf_op jit(solution)/shard_map/dot_general | solution.py:22
  30.9 0.0 reduce-scatter.2.cloned.1.call-update
  30.9 0.0 all-gather.6.cloned.1.call-start
  31.0 29.2 %reduce-scatter.2.cloned.1.call-done = f32[32,2048]{1,0:T(8,128)} async-done(((f32[128,2048]{1,0:T(8,128)}), f32[32,2048]{1,0:T(8,128)}) %reduce-scatter.2.cloned.1.call-update) | async-done | bytes 262160 | tf_op jit(solution)/shard_map/reduce_scatter | solution.py:23
  60.1 0.0 all-gather.6.cloned.1.call-update
  60.1 0.0 all-gather.4.cloned.1.call-start
  60.2 26.8 %all-gather.6.cloned.1.call-done = f32[128,2048]{1,0:T(8,128)} async-done(((f32[32,2048]{1,0:T(8,128)}), f32[128,2048]{1,0:T(8,128)}) %all-gather.6.cloned.1.call-update) | async-done | bytes 1048592 | tf_op jit(solution)/shard_map/all_gather | solution.py:24
  87.0 1.3 reduce_sum.18
  88.3 0.0 copy-done.3
  88.3 0.0 copy-done.4
  88.3 0.0 copy-start.1
  88.3 1.0 add_divide_fusion
  89.4 0.0 all-gather.4.cloned.1.call-update
  89.4 0.0 copy-start.2
  89.4 5.4 %copy.12 = f32[512,2048]{0,1:T(8,128)} copy(f32[512,2048]{1,0:T(8,128)} %param.9) | data formatting | bytes 8388608 | tf_op args[3]
  94.8 0.0 copy-done.1
  94.8 22.7 %all-gather.4.cloned.1.call-done = f32[128,2048]{1,0:T(8,128)} async-done(((f32[32,2048]{1,0:T(8,128)}), f32[128,2048]{1,0:T(8,128)}) %all-gather.4.cloned.1.call-update) | async-done | bytes 1048592 | tf_op jit(solution)/shard_map/all_gather | solution.py:28
  117.5 0.0 copy-done.2
  117.5 6.0 %multiply_reduce_fusion = (f32[]{:T(128)}, f32[2048,512]{1,0:T(8,128)}) fusion(f32[128,2048]{1,0:T(8,128)} %all-gather.4.cloned.1.call-done, bf16[512,128]{1,0:T(8,128)(2,1)S(1)} %copy-done.2), kind=kOutput, calls=%fused_computation.2 | convolution fusion | flops 1612709888 | bytes 5373956 | tf_op jit(solution)/shard_map/dot_general | solution.py:29
  123.5 15.3 %psum.7 = f32[]{:T(128)} all-reduce(f32[]{:T(128)} %get-tuple-element.18), channel_id=1, replica_groups=mesh['fs'=4,'rep'=4,'tp'=2] {'fs','tp'}, use_global_device_ids=true, to_apply=%region_3.0 | all-reduce | flops 1 | bytes 8 | tf_op jit(solution)/shard_map/psum | solution.py:30
  139.5 8.3 %fusion.4 = (bf16[512,2048]{0,1:T(8,128)(2,1)S(1)}, f32[512,2048]{0,1:T(8,128)}, f32[512,2048]{0,1:T(8,128)}) fusion(f32[512,2048]{0,1:T(8,128)} %copy.12, f32[2048,512]{1,0:T(8,128)} %get-tuple-element.19, f32[]{:T(128)S(6)} %add.27), kind=kLoop, calls=%fused_computation.12 | loop fusion | flops 4194304 | bytes 18874372 | tf_op jit(solution)/shard_map/convert_element_type | solution.py:34
  147.7 2.4 %copy.15 = bf16[512,2048]{1,0:T(8,128)(2,1)} copy(bf16[512,2048]{0,1:T(8,128)(2,1)S(1)} %get-tuple-element.12) | data formatting | bytes 4194304
  150.1 5.3 %copy.14 = f32[512,2048]{1,0:T(8,128)} copy(f32[512,2048]{0,1:T(8,128)} %get-tuple-element.13) | data formatting | bytes 8388608
  155.4 5.3 %copy.13 = f32[512,2048]{1,0:T(8,128)} copy(f32[512,2048]{0,1:T(8,128)} %get-tuple-element.14) | data formatting | bytes 8388608
Async XLA Ops:
  7.2 52.9 %reduce-scatter.2.cloned.1.call-start = ((), (), s32[]{:S(2)}) async-start(), calls=%async_computation.1 | async-start | bytes 1310720 | tf_op jit(solution)/shard_map/reduce_scatter | solution.py:23
  7.2 21.2 %copy-start = (bf16[1024,2048]{1,0:T(8,128)(2,1)S(1)}, bf16[1024,2048]{1,0:T(8,128)(2,1)}, u32[]{:S(2)}) copy-start(bf16[1024,2048]{1,0:T(8,128)(2,1)} %param.7) | copy-start | bytes 12582916
  29.1 59.2 %copy-start.3 = (f32[32,2048]{1,0:T(8,128)S(1)}, f32[32,2048]{1,0:T(8,128)}, u32[]{:S(2)}) copy-start(f32[32,2048]{1,0:T(8,128)} %param.11) | copy-start | bytes 786436
  29.1 59.1 %copy-start.4 = (f32[32,2048]{1,0:T(8,128)S(1)}, f32[32,2048]{1,0:T(8,128)}, u32[]{:S(2)}) copy-start(f32[32,2048]{1,0:T(8,128)} %param.10) | copy-start | bytes 786436
  30.9 56.1 %all-gather.6.cloned.1.call-start = ((), (), s32[]{:S(2)}) async-start(), calls=%async_computation.3 | async-start | bytes 1310720 | tf_op jit(solution)/shard_map/all_gather | solution.py:24
  60.1 57.4 %all-gather.4.cloned.1.call-start = ((), (), s32[]{:S(2)}) async-start(), calls=%async_computation.2 | async-start | bytes 1310720 | tf_op jit(solution)/shard_map/all_gather | solution.py:28
  88.3 6.5 %copy-start.1 = (f32[32,2048]{1,0:T(8,128)}, f32[32,2048]{1,0:T(8,128)S(1)}, u32[]{:S(2)}) copy-start(f32[32,2048]{1,0:T(8,128)S(1)} %reduce_sum.18) | copy-start | bytes 786436
  89.4 28.1 %copy-start.2 = (bf16[512,128]{1,0:T(8,128)(2,1)S(1)}, bf16[512,128]{1,0:T(8,128)(2,1)}, u32[]{:S(2)}) copy-start(bf16[512,128]{1,0:T(8,128)(2,1)} %param.8) | copy-start | bytes 393220
Sparse Core Ops, SparseCore 0:
  31.0 29.0 reduce-scatter.1
  62.0 24.9 all-gather.5
  89.5 27.9 all-gather.3
